TPU v7x, 32 devices: a whole 2x2x4 slice. The times are simulated.
32 devices in a mesh: sp: 16 (over z, y, core), tp: 2 (over x).
Axes of the slice: x: 2, y: 2, z: 4, core: 2. Of those that a mesh axis runs over, the one named last changes fastest.
Arguments:
- inputs: bfloat16 [2, 2048, 1024], P(None, 'sp'), may hold values from -6 to 6
- queries: bfloat16 [2, 2048, 4, 128], P(None, 'sp', 'tp'), may hold values from -6 to 6
- values: bfloat16 [2, 2048, 4, 256], P(None, 'sp', 'tp'), may hold values from -6 to 6
- out_grad: bfloat16 [2, 2048, 4, 256], P(None, 'sp', 'tp'), may hold values from -6 to 6
- key_weight: bfloat16 [1024, 4, 128], P(None, 'tp'), may hold values from -6 to 6
- decay_ahead: float32 [4], P('tp'), may hold values from -2.9 to 2.2
- decay_behind: float32 [4], P('tp'), may hold values from -2.9 to 2.2
Outputs:
- query_grad: bfloat16 [2, 2048, 4, 128], P(None, 'sp', 'tp')
- value_grad: bfloat16 [2, 2048, 4, 256], P(None, 'sp', 'tp')
- input_grad: bfloat16 [2, 2048, 1024], P('tp', 'sp')
- weight_grad: float32 [1024, 4, 128], P('sp', 'tp')
- decay_grad: float32 [2, 4], P(None, 'tp')
All inputs are finite; a program needn't handle non-finite values.
Results may differ from a plain program's by a relative error of at most 0.015.
Values may be sent and summed in bfloat16 or wider, within the bound.
A program may use at most 256 MiB of HBM per device.

v0:
```python
import math
import jax
import jax.numpy as jnp
from jax import lax
from jax.sharding import PartitionSpec as P

HIGHEST = lax.Precision.HIGHEST


def prefix(value, axis, join, neutral, backward):
    count, mine = (lax.axis_size(axis), lax.axis_index(axis))
    pieces = jax.tree.map(lambda part: lax.all_gather(part, axis), value)
    if backward:
        pieces = jax.tree.map(lambda part: part[::-1], pieces)
        mine = count - 1 - mine
    subtotal = jax.tree.map(
        lambda part, zero: jnp.full_like(part, 0) + jnp.asarray(zero, part.dtype), value, neutral
    )

    def step(position, subtotal):
        longer = join(subtotal, jax.tree.map(lambda part: part[position], pieces))
        return jax.tree.map(lambda new, old: jnp.where(position < mine, new, old), longer, subtotal)

    return lax.fori_loop(0, count - 1, step, subtotal)


def own_rows(contribution, rows, axis):
    whole = contribution(jnp.int32(0), rows * lax.axis_size(axis))
    return lax.psum_scatter(whole, axis, scatter_dimension=0, tiled=True)


def summed_rows(product, rows, axis):
    everything = product(jnp.int32(0), lax.axis_size(axis) * rows)
    own = lax.psum_scatter(everything.astype(jnp.bfloat16), axis, scatter_dimension=0, tiled=True)
    return own.astype(jnp.float32)


def link_states(earlier, later):
    return (
        earlier[0] * later[0],
        later[0] * earlier[1] + later[1],
        earlier[2] * later[2],
        later[2] * earlier[3] + later[3],
    )


def shards(inputs, queries, values, out_grad, key_weight, decay_ahead, decay_behind):
    batch_seqs, length, in_width = inputs.shape
    devices = lax.axis_size("sp")
    my_index = lax.axis_index("sp").astype(jnp.float32)
    all_tokens = length * devices
    key_scale = 1.0 / math.sqrt(in_width * queries.shape[3] * all_tokens)
    rate_ahead = jax.nn.log_sigmoid(decay_ahead) / all_tokens
    rate_behind = jax.nn.log_sigmoid(decay_behind) / all_tokens
    key_raw = jnp.einsum(
        "bld,dhk->blhk", inputs, key_weight, preferred_element_type=jnp.float32
    ).astype(jnp.bfloat16)
    keys = key_raw.astype(jnp.float32) * key_scale
    query_wide = queries.astype(jnp.float32)
    value_wide = values.astype(jnp.float32)
    grad_wide = out_grad.astype(jnp.float32)
    offsets = jnp.arange(length, dtype=jnp.float32)
    distance = offsets[:, None] - offsets[None, :]
    mask_ahead = jnp.where(
        distance[None] >= 0, jnp.exp(distance[None] * rate_ahead[:, None, None]), 0.0
    )
    mask_behind = jnp.where(
        distance[None] <= 0, jnp.exp(-distance[None] * rate_behind[:, None, None]), 0.0
    )
    mask_both = (mask_ahead + mask_behind)[None]
    keep_ahead = jnp.exp((length - 1.0 - offsets)[:, None] * rate_ahead[None])[None, :, :, None]
    keep_behind = jnp.exp(offsets[:, None] * rate_behind[None])[None, :, :, None]
    reach_ahead = jnp.exp((offsets + 1.0)[:, None] * rate_ahead[None])[None, :, :, None]
    reach_behind = jnp.exp((length - offsets)[:, None] * rate_behind[None])[None, :, :, None]
    scores = (
        jnp.einsum("bthk,bshk->bhts", queries, key_raw, preferred_element_type=jnp.float32)
        * key_scale
    )
    grad_scores = jnp.einsum(
        "bthv,bshv->bhts", out_grad, values, preferred_element_type=jnp.float32
    )
    sums_ahead = jnp.einsum("bshk,bshv->bhkv", keys * keep_ahead, value_wide, precision=HIGHEST)
    sums_behind = jnp.einsum("bshk,bshv->bhkv", keys * keep_behind, value_wide, precision=HIGHEST)
    pulls_ahead = jnp.einsum(
        "bthk,bthv->bhkv", query_wide * reach_ahead, grad_wide, precision=HIGHEST
    )
    pulls_behind = jnp.einsum(
        "bthk,bthv->bhkv", query_wide * reach_behind, grad_wide, precision=HIGHEST
    )
    span_ahead = jnp.exp(length * rate_ahead).reshape(1, -1, 1, 1)
    span_behind = jnp.exp(length * rate_behind).reshape(1, -1, 1, 1)
    unit_span = jnp.ones_like(span_ahead)
    zero_state = jnp.zeros_like(sums_ahead)
    upward = prefix(
        (span_ahead, sums_ahead, span_behind, pulls_behind),
        "sp",
        link_states,
        (unit_span, zero_state, unit_span, zero_state),
        False,
    )
    downward = prefix(
        (span_behind, sums_behind, span_ahead, pulls_ahead),
        "sp",
        link_states,
        (unit_span, zero_state, unit_span, zero_state),
        True,
    )
    state_ahead, pull_behind = (upward[1], upward[3])
    state_behind, pull_ahead = (downward[1], downward[3])
    out_ahead = jnp.einsum(
        "bhts,bshv->bthv", scores * mask_ahead[None], value_wide, precision=HIGHEST
    )
    out_ahead = out_ahead + jnp.einsum(
        "bthk,bhkv->bthv", query_wide * reach_ahead, state_ahead, precision=HIGHEST
    )
    out_behind = jnp.einsum(
        "bhts,bshv->bthv", scores * mask_behind[None], value_wide, precision=HIGHEST
    )
    out_behind = out_behind + jnp.einsum(
        "bthk,bhkv->bthv", query_wide * reach_behind, state_behind, precision=HIGHEST
    )
    grad_q = jnp.einsum("bhts,bshk->bthk", grad_scores * mask_both, keys, precision=HIGHEST)
    grad_q = grad_q + reach_ahead * jnp.einsum(
        "bthv,bhkv->bthk", grad_wide, state_ahead, precision=HIGHEST
    )
    grad_q = grad_q + reach_behind * jnp.einsum(
        "bthv,bhkv->bthk", grad_wide, state_behind, precision=HIGHEST
    )
    grad_k_ahead = jnp.einsum(
        "bhts,bthk->bshk", grad_scores * mask_ahead[None], query_wide, precision=HIGHEST
    )
    grad_k_ahead = grad_k_ahead + keep_ahead * jnp.einsum(
        "bshv,bhkv->bshk", value_wide, pull_ahead, precision=HIGHEST
    )
    grad_k_behind = jnp.einsum(
        "bhts,bthk->bshk", grad_scores * mask_behind[None], query_wide, precision=HIGHEST
    )
    grad_k_behind = grad_k_behind + keep_behind * jnp.einsum(
        "bshv,bhkv->bshk", value_wide, pull_behind, precision=HIGHEST
    )
    grad_v = jnp.einsum("bhts,bthv->bshv", scores * mask_both, grad_wide, precision=HIGHEST)
    grad_v = grad_v + keep_ahead * jnp.einsum(
        "bshk,bhkv->bshv", keys, pull_ahead, precision=HIGHEST
    )
    grad_v = grad_v + keep_behind * jnp.einsum(
        "bshk,bhkv->bshv", keys, pull_behind, precision=HIGHEST
    )
    positions = (my_index * length + offsets)[None, :, None]
    out_dot_ahead = jnp.sum(positions * jnp.sum(out_ahead * grad_wide, axis=3), axis=(0, 1))
    key_dot_ahead = jnp.sum(positions * jnp.sum(keys * grad_k_ahead, axis=3), axis=(0, 1))
    out_dot_behind = jnp.sum(positions * jnp.sum(out_behind * grad_wide, axis=3), axis=(0, 1))
    key_dot_behind = jnp.sum(positions * jnp.sum(keys * grad_k_behind, axis=3), axis=(0, 1))
    local_sums = jnp.stack([out_dot_ahead - key_dot_ahead, key_dot_behind - out_dot_behind])
    rate_sums = lax.psum(local_sums, "sp")
    slopes = jnp.stack([jax.nn.sigmoid(-decay_ahead), jax.nn.sigmoid(-decay_behind)]) / all_tokens
    decay_grad = rate_sums * slopes
    key_grad_raw = ((grad_k_ahead + grad_k_behind) * key_scale).astype(jnp.bfloat16)

    def weight_rows(start, row_count):
        piece = lax.dynamic_slice_in_dim(inputs, start, row_count, 2)
        return jnp.einsum("bld,blhk->dhk", piece, key_grad_raw, preferred_element_type=jnp.float32)

    weight_grad = own_rows(weight_rows, in_width // devices, "sp")

    def input_rows(start, row_count):
        piece = lax.dynamic_slice_in_dim(key_grad_raw, start, row_count, 0)
        return jnp.einsum("blhk,dhk->bld", piece, key_weight, preferred_element_type=jnp.float32)

    input_grad = summed_rows(input_rows, batch_seqs // lax.axis_size("tp"), "tp").astype(
        jnp.bfloat16
    )
    return (
        grad_q.astype(jnp.bfloat16),
        grad_v.astype(jnp.bfloat16),
        input_grad,
        weight_grad,
        decay_grad,
    )


def solution(mesh):
    in_specs = (
        P(None, "sp", None),
        P(None, "sp", "tp", None),
        P(None, "sp", "tp", None),
        P(None, "sp", "tp", None),
        P(None, "tp", None),
        P("tp"),
        P("tp"),
    )
    out_specs = (
        P(None, "sp", "tp", None),
        P(None, "sp", "tp", None),
        P("tp", "sp", None),
        P("sp", "tp", None),
        P(None, "tp"),
    )
    return jax.shard_map(shards, mesh=mesh, in_specs=in_specs, out_specs=out_specs, check_vma=False)
```

profile of v0, /device:TPU:0, one launch (start us, length us, event | category | flops | bytes accessed | tf_op | source)
XLA Modules:
  0.0 462.7 jit_solution(7390019577858132643)
XLA Ops:
  7.3 1.4 copy.106
  8.7 1.3 broadcast_multiply_fusion.3
  10.9 2.1 fusion.41
  14.8 2.1 fusion.37
  17.1 2.1 fusion.40
  19.2 2.1 fusion.36
  21.5 1.3 fusion.92
  23.7 36.6 %all-reduce.3 = (f32[32]{0:T(128)S(1)}, f32[32]{0:T(128)S(1)}) all-reduce(f32[32]{0:T(128)S(1)} %exponential_dynamic-update-slice_fusion, f32[32]{0:T(128)S(1)} %exponential_dynamic-update-slice_fusion.1), channel_id=4, replica_groups=mesh['sp'=16,'tp'=2] {'sp'}, use_global_device_ids=true, to_apply=%add.1 | all-reduce | flops 64 | bytes 512
  61.8 1.6 broadcast_multiply_fusion
  63.4 1.7 copy.122
  65.1 1.7 copy.144
  70.5 19.9 %all-gather.15.cloned.1.call-done = f32[32,2,128,256]{3,2,1,0:T(8,128)} async-done(((f32[2,2,128,256]{3,2,1,0:T(8,128)}), f32[32,2,128,256]{3,2,1,0:T(8,128)}) %all-gather.15.cloned.1.call-update) | async-done | bytes 8388624 | tf_op jit(solution)/shard_map/all_gather | solution.py:12
  90.5 7.6 %rev.13 = f32[16,2,2,128,256]{4,3,2,1,0:T(8,128)} reverse(f32[16,2,2,128,256]{4,3,2,1,0:T(8,128)} %bitcast.160), dimensions={0} | reverse | bytes 16777216 | tf_op jit(solution)/shard_map/rev | solution.py:14
  98.1 67.5 %all-gather.17.cloned.1.call-done = f32[32,2,128,256]{3,2,1,0:T(8,128)} async-done(((f32[2,2,128,256]{3,2,1,0:T(8,128)}), f32[32,2,128,256]{3,2,1,0:T(8,128)}) %all-gather.17.cloned.1.call-update) | async-done | bytes 8388624 | tf_op jit(solution)/shard_map/all_gather | solution.py:12
  165.6 7.6 %rev.15 = f32[16,2,2,128,256]{4,3,2,1,0:T(8,128)} reverse(f32[16,2,2,128,256]{4,3,2,1,0:T(8,128)} %bitcast.161), dimensions={0} | reverse | bytes 16777216 | tf_op jit(solution)/shard_map/rev | solution.py:14
  173.1 42.3 %while.33 = (s32[]{:T(128)}, f32[2,2,128,256]{3,2,1,0:T(8,128)S(1)}, f32[2,2,128,256]{3,2,1,0:T(8,128)S(1)}, s32[]{:T(128)}, f32[16,1,2,1,1]{2,4,3,1,0:T(1,128)}...) while((s32[]{:T(128)}, ...), condition=%wide.region_3.4_spmd.clone, body=%wide.region_2.3_spmd.clone.sunk | while | flops 1048580 | bytes 3145917 | solution.py:24
  174.4 1.5 fusion.118
  177.2 1.5 fusion.118
  180.0 1.5 fusion.118
  182.7 1.5 fusion.118
  185.5 1.5 fusion.118
  188.3 1.5 fusion.118
  191.1 1.5 fusion.118
  193.9 1.5 fusion.118
  196.8 1.5 fusion.118
  199.5 1.8 fusion.118
  202.6 1.5 fusion.118
  205.4 1.5 fusion.118
  208.2 1.5 fusion.118
  211.1 1.5 fusion.118
  213.9 1.5 fusion.118
  216.5 1.4 convolution_bitcast_fusion.2
  218.0 22.7 %all-gather.11.cloned.1.call-done = f32[32,2,128,256]{3,2,1,0:T(8,128)} async-done(((f32[2,2,128,256]{3,2,1,0:T(8,128)}), f32[32,2,128,256]{3,2,1,0:T(8,128)}) %all-gather.11.cloned.1.call-update) | async-done | bytes 8388624 | tf_op jit(solution)/shard_map/all_gather | solution.py:12
  240.6 74.9 %all-gather.13.cloned.1.call-done = f32[32,2,128,256]{3,2,1,0:T(8,128)} async-done(((f32[2,2,128,256]{3,2,1,0:T(8,128)}), f32[32,2,128,256]{3,2,1,0:T(8,128)}) %all-gather.13.cloned.1.call-update) | async-done | bytes 8388624 | tf_op jit(solution)/shard_map/all_gather | solution.py:12
  315.6 23.2 %while.32 = (s32[]{:T(128)}, f32[2,2,128,256]{3,2,1,0:T(8,128)S(1)}, f32[2,2,128,256]{3,2,1,0:T(8,128)S(1)}, s32[]{:T(128)}, f32[16,1,2,1,1]{2,4,3,1,0:T(1,128)S...) while((s32[]{:T(128)}, ...), condition=%wide.region_1.2_spmd.clone, body=%wide.region_0.1_spmd.clone.sunk | while | flops 1048580 | bytes 3145917 | solution.py:24
  315.6 1.5 fusion.115
  317.2 1.5 fusion.115
  318.7 1.5 fusion.115
  320.3 1.5 fusion.115
  321.8 1.5 fusion.115
  323.3 1.5 fusion.115
  324.9 1.5 fusion.115
  326.4 1.5 fusion.115
  328.0 1.5 fusion.115
  329.5 1.5 fusion.115
  331.1 1.5 fusion.115
  332.6 1.5 fusion.115
  334.2 1.5 fusion.115
  335.7 1.5 fusion.115
  337.2 1.5 fusion.115
  338.8 1.1 fusion.20
  341.3 1.8 fusion.38
  343.1 1.3 convolution_bitcast_fusion
  344.4 2.2 copy.136
  347.4 1.6 fusion.18
  349.0 1.4 fusion.19
  351.7 31.6 %psum.7 = f32[2,2]{1,0:T(2,128)S(1)} all-reduce(f32[2,2]{1,0:T(2,128)S(1)} %pad_maximum_fusion), channel_id=1, replica_groups=mesh['sp'=16,'tp'=2] {'sp'}, use_global_device_ids=true, to_apply=%region_14.15 | all-reduce | flops 4 | bytes 32 | tf_op jit(solution)/shard_map/psum | solution.py:154
  383.3 1.7 fusion.28
  385.8 2.2 fusion.8
  389.3 1.3 fusion.17
  391.5 1.3 fusion.83
  392.8 46.6 %all-reduce.6.cloned.1.call-done = f32[1024,2,128]{2,1,0:T(2,128)} async-done(((f32[1024,2,128]{2,1,0:T(2,128)}), f32[1024,2,128]{2,1,0:T(2,128)}) %all-reduce.6.cloned.1.call-update) | async-done | bytes 1048592
  439.4 1.5 constant_dynamic-slice_fusion.4
  440.9 15.0 %reduce-scatter.2.cloned.1.call-done = bf16[1,128,1024]{2,1,0:T(8,128)(2,1)} async-done(((bf16[2,128,1024]{2,1,0:T(8,128)(2,1)}), bf16[1,128,1024]{2,1,0:T(8,128)(2,1)}) %reduce-scatter.2.cloned.1.call-update) | async-done | bytes 262160 | tf_op jit(solution)/shard_map/reduce_scatter | solution.py:34
  (137 shorter events, 34.8 us)
Async XLA Ops:
  7.2 2.8 copy-start
  7.2 62.4 %copy-start.2 = (bf16[2,128,2,256]{3,2,1,0:T(2,128)(2,1)S(1)}, bf16[2,128,2,256]{3,2,1,0:T(2,128)(2,1)}, u32[]{:S(2)}) copy-start(bf16[2,128,2,256]{3,2,1,0:T(2,128)(2,1)} %param.13) | copy-start | bytes 786436
  7.2 62.4 %copy-start.1 = (bf16[2,128,2,256]{3,2,1,0:T(2,128)(2,1)S(1)}, bf16[2,128,2,256]{3,2,1,0:T(2,128)(2,1)}, u32[]{:S(2)}) copy-start(bf16[2,128,2,256]{3,2,1,0:T(2,128)(2,1)} %param.14) | copy-start | bytes 786436
  7.2 83.3 %all-gather.15.cloned.1.call-start = ((), (), s32[]{:S(2)}) async-start(), calls=%async_computation.4 | async-start | bytes 8912896 | tf_op jit(solution)/shard_map/all_gather | solution.py:12
  9.9 11.6 %copy-start.12 = (f32[2]{0:T(128)}, f32[2]{0:T(128)S(1)}, u32[]{:S(2)}) copy-start(f32[2]{0:T(128)S(1)} %get-tuple-element.478) | copy-start | bytes 28
  9.9 11.6 %copy-start.13 = (f32[2]{0:T(128)}, f32[2]{0:T(128)S(1)}, u32[]{:S(2)}) copy-start(f32[2]{0:T(128)S(1)} %get-tuple-element.450) | copy-start | bytes 28
  10.9 10.5 %copy-start.8 = (f32[128,2]{0,1:T(2,128)}, f32[128,2]{0,1:T(2,128)S(1)}, u32[]{:S(2)}) copy-start(f32[128,2]{0,1:T(2,128)S(1)} %get-tuple-element.470) | copy-start | bytes 3076
  13.1 152.5 %all-gather.17.cloned.1.call-start = ((), (), s32[]{:S(2)}) async-start(), calls=%async_computation.5 | async-start | bytes 8912896 | tf_op jit(solution)/shard_map/all_gather | solution.py:12
  14.8 6.6 %copy-start.6 = (f32[128,2]{0,1:T(2,128)}, f32[128,2]{0,1:T(2,128)S(1)}, u32[]{:S(2)}) copy-start(f32[128,2]{0,1:T(2,128)S(1)} %get-tuple-element.467) | copy-start | bytes 3076
  17.0 223.6 %all-gather.11.cloned.1.call-start = ((), (), s32[]{:S(2)}) async-start(), calls=%async_computation.2 | async-start | bytes 8912896 | tf_op jit(solution)/shard_map/all_gather | solution.py:12
  19.2 296.4 %all-gather.13.cloned.1.call-start = ((), (), s32[]{:S(2)}) async-start(), calls=%async_computation.3 | async-start | bytes 8912896 | tf_op jit(solution)/shard_map/all_gather | solution.py:12
  21.4 418.0 %all-reduce.6.cloned.1.call-start = ((), (), s32[]{:S(2)}) async-start(), calls=%async_computation.6 | async-start | bytes 2097152
  173.1 42.3 %copy-start.9 = (f32[128,2]{0,1:T(2,128)S(1)}, f32[128,2]{0,1:T(2,128)}, u32[]{:S(2)}) copy-start(f32[128,2]{0,1:T(2,128)} %copy-done.8) | copy-start | bytes 3076
  315.6 25.4 %copy-start.3 = (f32[2,2,128,128]{3,2,1,0:T(8,128)S(1)}, f32[2,2,128,128]{3,2,1,0:T(8,128)}, u32[]{:S(2)}) copy-start(f32[2,2,128,128]{3,2,1,0:T(8,128)} %fusion.72) | copy-start | bytes 786436
  315.6 25.4 %copy-start.5 = (f32[2,128,128]{2,1,0:T(8,128)S(1)}, f32[2,128,128]{2,1,0:T(8,128)}, u32[]{:S(2)}) copy-start(f32[2,128,128]{2,1,0:T(8,128)} %get-tuple-element.459) | copy-start | bytes 393220
  338.7 8.0 %copy-start.7 = (f32[128,2]{0,1:T(2,128)S(1)}, f32[128,2]{0,1:T(2,128)}, u32[]{:S(2)}) copy-start(f32[128,2]{0,1:T(2,128)} %copy-done.6) | copy-start | bytes 3076
  338.8 8.6 %copy-start.4 = (f32[2,2,128,128]{2,3,1,0:T(8,128)S(1)}, f32[2,2,128,128]{2,3,1,0:T(8,128)}, u32[]{:S(2)}) copy-start(f32[2,2,128,128]{2,3,1,0:T(8,128)} %convolution_bitcast_fusion.16) | copy-start | bytes 786436
  339.9 48.1 %copy-start.10 = (f32[128,2]{0,1:T(2,128)S(1)}, f32[128,2]{0,1:T(2,128)}, u32[]{:S(2)}) copy-start(f32[128,2]{0,1:T(2,128)} %get-tuple-element.468) | copy-start | bytes 3076
  340.9 47.7 %copy-start.11 = (f32[128,2]{0,1:T(2,128)S(1)}, f32[128,2]{0,1:T(2,128)}, u32[]{:S(2)}) copy-start(f32[128,2]{0,1:T(2,128)} %get-tuple-element.461) | copy-start | bytes 3076
  346.7 109.2 %reduce-scatter.2.cloned.1.call-start = ((), (), s32[]{:S(2)}) async-start(), calls=%async_computation.1 | async-start | bytes 786432 | tf_op jit(solution)/shard_map/reduce_scatter | solution.py:34
Sparse Core Ops, SparseCore 0:
  13.2 77.2 all-gather.14
  92.6 72.8 all-gather.16
  167.7 72.8 all-gather.10
  242.6 72.8 all-gather.12
  346.8 92.5 all-reduce.5
  442.1 13.7 reduce-scatter.1
where the time goes:
time: 464 us; the launch traced here: 463 us
  waiting for transfers between devices  247 us (53%)
  blocking collectives  68.2 us (15%)
  other arithmetic  51.9 us (11%)
  local copies, waits for them, and re-layouts  49.5 us (11%)
  matrix products  29.3 us (6%)
  between operations  15.8 us (3%)
    all_gather x4, waiting for transfers between devices, prefix(): pieces = jax.tree.map(lambda part: lax.all_gather(part, axis), value)  185 us
    unnamed x7, waiting for transfers between devices  46.7 us
    select_n x30, other arithmetic, step(): jnp.where(position < mine, new, old)  44.9 us
    unnamed x1, blocking collectives  36.6 us
    psum x1, blocking collectives, shards(): rate_sums = lax.psum(local_sums, 'sp')  31.6 us
    rev x4, local copies, waits for them, and re-layouts, prefix(): pieces = jax.tree.map(lambda part: part[::-1], pieces)  16.4 us
    reduce_scatter x1, waiting for transfers between devices, summed_rows(): lax.psum_scatter(everything.astype(jnp.bfloat16), axis, scatter_dimension...  15 us
    mul x30, local copies, waits for them, and re-layouts, link_states(): later[0] * earlier[1] + later[1]  9.94 us
  transfers between devices with their start and end apart: 6, of which 6 were waited for; matrix products, arithmetic and copies ran while one was open for 20% of the time, Pallas kernels for 0%

commit v1 on v0

--- a/solution.py
+++ b/solution.py
@@ -151,7 +151,8 @@
     out_dot_behind = jnp.sum(positions * jnp.sum(out_behind * grad_wide, axis=3), axis=(0, 1))
     key_dot_behind = jnp.sum(positions * jnp.sum(keys * grad_k_behind, axis=3), axis=(0, 1))
     local_sums = jnp.stack([out_dot_ahead - key_dot_ahead, key_dot_behind - out_dot_behind])
-    rate_sums = lax.psum(local_sums, "sp")
+    arr_next = lax.all_gather(local_sums, "sp")
+    rate_sums = jnp.sum(arr_next, axis=0)
     slopes = jnp.stack([jax.nn.sigmoid(-decay_ahead), jax.nn.sigmoid(-decay_behind)]) / all_tokens
     decay_grad = rate_sums * slopes
     key_grad_raw = ((grad_k_ahead + grad_k_behind) * key_scale).astype(jnp.bfloat16)

time: 464 us -> 494 us (1.065)
  waiting for transfers between devices: 247 us -> 278 us
  blocking collectives: 68.2 us -> 55.7 us
  local copies, waits for them, and re-layouts: 49.5 us -> 58.3 us
    psum x1 -> x0, blocking collectives: 31.6 us -> none  [shards(): rate_sums = lax.psum(local_sums, 'sp')]
    all_gather x0 -> x1, blocking collectives: none -> 19.1 us  [shards(): arr_next = lax.all_gather(local_sums, 'sp')]
    all_gather x4, waiting for transfers between devices: 185 us -> 202 us  [prefix(): pieces = jax.tree.map(lambda part: lax.all_gather(part, axis), value)]
    unnamed x7, waiting for transfers between devices: 46.7 us -> 60.7 us
    mul x30, local copies, waits for them, and re-layouts: 9.63 us -> 17.5 us  [link_states(): later[2] * earlier[3] + later[3]]
  transfers between devices with their start and end apart: 6 -> 6, of which waited for: 6 -> 6; matrix products, arithmetic and copies ran while one was open for 20% -> 15% of each run, Pallas kernels for 0% -> 0%
where the time goes in v1:
time: 494 us; the launch traced here: 492 us
  waiting for transfers between devices  278 us (56%)
  local copies, waits for them, and re-layouts  58.3 us (12%)
  blocking collectives  55.7 us (11%)
  other arithmetic  51.8 us (10%)
  matrix products  32.2 us (7%)
  between operations  15.8 us (3%)
    all_gather x4, waiting for transfers between devices, prefix(): pieces = jax.tree.map(lambda part: lax.all_gather(part, axis), value)  202 us
    unnamed x7, waiting for transfers between devices  60.7 us
    select_n x30, other arithmetic, step(): jnp.where(position < mine, new, old)  44.6 us
    unnamed x1, blocking collectives  36.6 us
    all_gather x1, blocking collectives, shards(): arr_next = lax.all_gather(local_sums, 'sp')  19.1 us
    mul x30, local copies, waits for them, and re-layouts, link_states(): later[2] * earlier[3] + later[3]  17.5 us
    rev x4, local copies, waits for them, and re-layouts, prefix(): pieces = jax.tree.map(lambda part: part[::-1], pieces)  16.4 us
    reduce_scatter x1, waiting for transfers between devices, summed_rows(): lax.psum_scatter(everything.astype(jnp.bfloat16), axis, scatter_dimension...  15 us
  transfers between devices with their start and end apart: 6, of which 6 were waited for; matrix products, arithmetic and copies ran while one was open for 15% of the time, Pallas kernels for 0%

profile of v1, /device:TPU:0, one launch (start us, length us, event | category | flops | bytes accessed | tf_op | source)
XLA Modules:
  0.0 492.3 jit_solution(453573500507484473)
XLA Ops:
  7.3 1.4 copy.106
  10.9 2.1 fusion.41
  13.8 2.1 fusion.40
  17.0 2.1 fusion.36
  19.2 2.1 fusion.37
  21.5 1.4 fusion.92
  23.8 36.6 %all-reduce.3 = (f32[32]{0:T(128)S(1)}, f32[32]{0:T(128)S(1)}) all-reduce(f32[32]{0:T(128)S(1)} %exponential_dynamic-update-slice_fusion, f32[32]{0:T(128)S(1)} %exponential_dynamic-update-slice_fusion.1), channel_id=4, replica_groups=mesh['sp'=16,'tp'=2] {'sp'}, use_global_device_ids=true, to_apply=%add.1 | all-reduce | flops 64 | bytes 512
  61.8 1.6 broadcast_multiply_fusion
  63.4 1.7 copy.122
  65.1 1.7 copy.144
  66.8 1.6 copy.137
  71.6 18.9 %all-gather.17.cloned.1.call-done = f32[32,2,128,256]{3,2,1,0:T(8,128)} async-done(((f32[2,2,128,256]{3,2,1,0:T(8,128)}), f32[32,2,128,256]{3,2,1,0:T(8,128)}) %all-gather.17.cloned.1.call-update) | async-done | bytes 8388624 | tf_op jit(solution)/shard_map/all_gather | solution.py:12
  90.5 7.6 %rev.13 = f32[16,2,2,128,256]{4,3,2,1,0:T(8,128)} reverse(f32[16,2,2,128,256]{4,3,2,1,0:T(8,128)} %bitcast.163), dimensions={0} | reverse | bytes 16777216 | tf_op jit(solution)/shard_map/rev | solution.py:14
  98.1 67.5 %all-gather.13.cloned.1.call-done = f32[32,2,128,256]{3,2,1,0:T(8,128)} async-done(((f32[2,2,128,256]{3,2,1,0:T(8,128)}), f32[32,2,128,256]{3,2,1,0:T(8,128)}) %all-gather.13.cloned.1.call-update) | async-done | bytes 8388624 | tf_op jit(solution)/shard_map/all_gather | solution.py:12
  165.6 75.1 %all-gather.15.cloned.1.call-done = f32[32,2,128,256]{3,2,1,0:T(8,128)} async-done(((f32[2,2,128,256]{3,2,1,0:T(8,128)}), f32[32,2,128,256]{3,2,1,0:T(8,128)}) %all-gather.15.cloned.1.call-update) | async-done | bytes 8388624 | tf_op jit(solution)/shard_map/all_gather | solution.py:12
  240.6 30.6 %while.32 = (s32[]{:T(128)}, f32[2,2,128,256]{3,2,1,0:T(8,128)S(1)}, f32[2,2,128,256]{3,2,1,0:T(8,128)S(1)}, s32[]{:T(128)}, f32[16,1,2,1,1]{2,4,3,1,0:T(1,128)S...) while((s32[]{:T(128)}, ...), condition=%wide.region_1.2_spmd.clone, body=%wide.region_0.1_spmd.clone.sunk | while | flops 1048580 | bytes 3145917 | solution.py:24
  241.1 1.5 fusion.115
  243.2 1.5 fusion.115
  245.2 1.5 fusion.115
  247.2 1.6 fusion.115
  249.3 1.5 fusion.115
  251.4 1.5 fusion.115
  253.4 1.5 fusion.115
  255.5 1.5 fusion.115
  257.5 1.5 fusion.115
  259.6 1.5 fusion.115
  261.6 1.5 fusion.115
  263.6 1.5 fusion.115
  265.7 1.5 fusion.115
  267.7 1.5 fusion.115
  269.7 1.5 fusion.115
  271.2 1.8 fusion.20
  273.0 2.1 fusion.16
  275.2 40.4 %all-gather.19.cloned.1.call-done = f32[32,2,128,256]{3,2,1,0:T(8,128)} async-done(((f32[2,2,128,256]{3,2,1,0:T(8,128)}), f32[32,2,128,256]{3,2,1,0:T(8,128)}) %all-gather.19.cloned.1.call-update) | async-done | bytes 8388624 | tf_op jit(solution)/shard_map/all_gather | solution.py:12
  315.6 7.6 %rev.15 = f32[16,2,2,128,256]{4,3,2,1,0:T(8,128)} reverse(f32[16,2,2,128,256]{4,3,2,1,0:T(8,128)} %bitcast.162), dimensions={0} | reverse | bytes 16777216 | tf_op jit(solution)/shard_map/rev | solution.py:14
  323.2 42.1 %while.33 = (s32[]{:T(128)}, f32[2,2,128,256]{3,2,1,0:T(8,128)S(1)}, f32[2,2,128,256]{3,2,1,0:T(8,128)S(1)}, s32[]{:T(128)}, f32[16,1,2,1,1]{2,4,3,1,0:T(1,128)}...) while((s32[]{:T(128)}, ...), condition=%wide.region_3.4_spmd.clone, body=%wide.region_2.3_spmd.clone.sunk | while | flops 1048580 | bytes 3145917 | solution.py:24
  324.5 1.5 fusion.118
  327.4 1.5 fusion.118
  330.1 1.5 fusion.118
  333.0 1.5 fusion.118
  335.7 1.5 fusion.118
  338.5 1.5 fusion.118
  341.4 1.5 fusion.118
  344.2 1.5 fusion.118
  346.9 1.5 fusion.118
  349.7 1.5 fusion.118
  352.5 1.5 fusion.118
  355.4 1.5 fusion.118
  358.2 1.5 fusion.118
  361.0 1.5 fusion.118
  363.7 1.5 fusion.118
  365.3 1.4 fusion.15
  367.1 1.3 fusion.21
  369.7 2.2 fusion.8
  371.9 1.3 convolution_bitcast_fusion
  374.3 2.2 copy.136
  379.2 1.7 fusion.28
  380.9 1.4 fusion.18
  382.3 1.6 fusion.17
  383.9 1.4 fusion.19
  388.0 19.1 %all-gather.7 = f32[16,2,2]{2,1,0:T(2,128)S(1)} all-gather(f32[1,2,2]{2,1,0:T(2,128)S(1)} %maximum_bitcast_fusion), channel_id=8, replica_groups=mesh['sp'=16,'tp'=2] {'sp'}, dimensions={0}, use_global_device_ids=true | all-gather | bytes 272 | tf_op jit(solution)/shard_map/all_gather | solution.py:154
  408.4 60.6 %all-reduce.6.cloned.1.call-done = f32[1024,2,128]{2,1,0:T(2,128)} async-done(((f32[1024,2,128]{2,1,0:T(2,128)}), f32[1024,2,128]{2,1,0:T(2,128)}) %all-reduce.6.cloned.1.call-update) | async-done | bytes 1048592
  469.0 1.5 constant_dynamic-slice_fusion.4
  470.5 15.0 %reduce-scatter.2.cloned.1.call-done = bf16[1,128,1024]{2,1,0:T(8,128)(2,1)} async-done(((bf16[2,128,1024]{2,1,0:T(8,128)(2,1)}), bf16[1,128,1024]{2,1,0:T(8,128)(2,1)}) %reduce-scatter.2.cloned.1.call-update) | async-done | bytes 262160 | tf_op jit(solution)/shard_map/reduce_scatter | solution.py:34
  (134 shorter events, 45.0 us)
Async XLA Ops:
  7.2 2.8 copy-start
  7.2 63.5 %copy-start.2 = (bf16[2,128,2,256]{3,2,1,0:T(2,128)(2,1)S(1)}, bf16[2,128,2,256]{3,2,1,0:T(2,128)(2,1)}, u32[]{:S(2)}) copy-start(bf16[2,128,2,256]{3,2,1,0:T(2,128)(2,1)} %param.13) | copy-start | bytes 786436
  7.2 63.5 %copy-start.1 = (bf16[2,128,2,256]{3,2,1,0:T(2,128)(2,1)S(1)}, bf16[2,128,2,256]{3,2,1,0:T(2,128)(2,1)}, u32[]{:S(2)}) copy-start(bf16[2,128,2,256]{3,2,1,0:T(2,128)(2,1)} %param.14) | copy-start | bytes 786436
  7.2 83.3 %all-gather.17.cloned.1.call-start = ((), (), s32[]{:S(2)}) async-start(), calls=%async_computation.4 | async-start | bytes 8912896 | tf_op jit(solution)/shard_map/all_gather | solution.py:12
  9.9 11.6 %copy-start.10 = (f32[2]{0:T(128)}, f32[2]{0:T(128)S(1)}, u32[]{:S(2)}) copy-start(f32[2]{0:T(128)S(1)} %get-tuple-element.478) | copy-start | bytes 28
  9.9 11.6 %copy-start.11 = (f32[2]{0:T(128)}, f32[2]{0:T(128)S(1)}, u32[]{:S(2)}) copy-start(f32[2]{0:T(128)S(1)} %get-tuple-element.450) | copy-start | bytes 28
  10.9 10.5 %copy-start.5 = (f32[128,2]{0,1:T(2,128)}, f32[128,2]{0,1:T(2,128)S(1)}, u32[]{:S(2)}) copy-start(f32[128,2]{0,1:T(2,128)S(1)} %get-tuple-element.470) | copy-start | bytes 3076
  13.1 152.5 %all-gather.13.cloned.1.call-start = ((), (), s32[]{:S(2)}) async-start(), calls=%async_computation.2 | async-start | bytes 8912896 | tf_op jit(solution)/shard_map/all_gather | solution.py:12
  13.8 7.6 %copy-start.7 = (f32[128,2]{0,1:T(2,128)}, f32[128,2]{0,1:T(2,128)S(1)}, u32[]{:S(2)}) copy-start(f32[128,2]{0,1:T(2,128)S(1)} %get-tuple-element.467) | copy-start | bytes 3076
  15.9 224.7 %all-gather.15.cloned.1.call-start = ((), (), s32[]{:S(2)}) async-start(), calls=%async_computation.3 | async-start | bytes 8912896 | tf_op jit(solution)/shard_map/all_gather | solution.py:12
  19.2 296.4 %all-gather.19.cloned.1.call-start = ((), (), s32[]{:S(2)}) async-start(), calls=%async_computation.5 | async-start | bytes 8912896 | tf_op jit(solution)/shard_map/all_gather | solution.py:12
  21.4 447.6 %all-reduce.6.cloned.1.call-start = ((), (), s32[]{:S(2)}) async-start(), calls=%async_computation.6 | async-start | bytes 2097152
  323.2 42.1 %copy-start.9 = (f32[128,2]{0,1:T(2,128)S(1)}, f32[128,2]{0,1:T(2,128)}, u32[]{:S(2)}) copy-start(f32[128,2]{0,1:T(2,128)} %get-tuple-element.461) | copy-start | bytes 3076
  323.2 43.9 %copy-start.3 = (f32[2,2,128,128]{3,2,1,0:T(8,128)S(1)}, f32[2,2,128,128]{3,2,1,0:T(8,128)}, u32[]{:S(2)}) copy-start(f32[2,2,128,128]{3,2,1,0:T(8,128)} %fusion.72) | copy-start | bytes 786436
  323.2 50.0 %copy-start.6 = (f32[128,2]{0,1:T(2,128)S(1)}, f32[128,2]{0,1:T(2,128)}, u32[]{:S(2)}) copy-start(f32[128,2]{0,1:T(2,128)} %copy-done.5) | copy-start | bytes 3076
  365.2 11.5 %copy-start.8 = (f32[128,2]{0,1:T(2,128)S(1)}, f32[128,2]{0,1:T(2,128)}, u32[]{:S(2)}) copy-start(f32[128,2]{0,1:T(2,128)} %copy-done.7) | copy-start | bytes 3076
  365.3 15.6 %copy-start.4 = (f32[2,2,128,128]{2,3,1,0:T(8,128)S(1)}, f32[2,2,128,128]{2,3,1,0:T(8,128)}, u32[]{:S(2)}) copy-start(f32[2,2,128,128]{2,3,1,0:T(8,128)} %convolution_bitcast_fusion.16) | copy-start | bytes 786436
  376.5 108.9 %reduce-scatter.2.cloned.1.call-start = ((), (), s32[]{:S(2)}) async-start(), calls=%async_computation.1 | async-start | bytes 786432 | tf_op jit(solution)/shard_map/reduce_scatter | solution.py:34
Sparse Core Ops, SparseCore 0:
  13.2 77.2 all-gather.16
  92.6 72.8 all-gather.12
  167.7 72.8 all-gather.14
  242.6 72.8 all-gather.18
  376.7 92.3 all-reduce.5
  471.7 13.7 reduce-scatter.1
